TPU v7x, 32 devices: a whole 2x2x4 slice. The times are simulated.
32 devices in a mesh: ep: 8 (over z, x), tp: 4 (over y, core).
Axes of the slice: x: 2, y: 2, z: 4, core: 2. Of those that a mesh axis runs over, the one named last changes fastest.
Arguments:
- tokens: bfloat16 [64, 2048], P('ep'), may hold values from -6 to 6
- mix_gain: bfloat16 [2048], replicated, may hold values from 0.099609375 to 1.8984375
- w_query: bfloat16 [2048, 512], P(None, 'tp'), may hold values from -0.125 to 0.125
- w_key: bfloat16 [2048, 512], P(None, 'tp'), may hold values from -0.125 to 0.125
- w_value: bfloat16 [2048, 512], P(None, 'tp'), may hold values from -0.125 to 0.125
- w_igate: bfloat16 [2048, 4], replicated, may hold values from -0.125 to 0.125
- w_fgate: bfloat16 [2048, 4], replicated, may hold values from -0.125 to 0.125
- forget_bias: float32 [4], replicated, may hold values from 0.5 to 4.5
- w_out: bfloat16 [512, 2048], P('tp'), may hold values from -0.25 to 0.25
- mem_state: float32 [64, 4, 16384], P('ep', 'tp'), may hold values from -0.75 to 0.75
- norm_state: float32 [64, 512], P('ep', 'tp'), may hold values from -0.75 to 0.75
- max_state: float32 [64, 4], P('ep', 'tp'), may hold values from -3 to 3
- ffn_gain: bfloat16 [2048], replicated, may hold values from 0.099609375 to 1.8984375
- route_ids: int32 [64, 2], P('ep'), may hold values from 0 to 7, all different within a row; in each aligned block of 8 rows (0 to 7, 8 to 15, ...) at most 3 rows name the same one
- route_weights: float32 [64, 2], P('ep'), may hold values from 0.1 to 1
- w_gate: bfloat16 [2048, 32768], P(None, ('ep', 'tp')), may hold values from -0.125 to 0.125
- w_up: bfloat16 [2048, 32768], P(None, ('ep', 'tp')), may hold values from -0.125 to 0.125
- w_down: bfloat16 [32768, 2048], P('ep', 'tp'), may hold values from -0.09375 to 0.09375
Outputs:
- out_tokens: bfloat16 [64, 2048], P('ep', 'tp')
- new_memory: float32 [64, 4, 16384], P('ep', 'tp')
- new_norm: float32 [64, 512], P('ep', 'tp')
- new_max: float32 [64, 4], P('ep', 'tp')
Inputs may be any that keep to these rules, and one draw needn't show every extreme that they name: `route_ids`: each row names 2 different experts; among the rows of one index of ep no expert is named more than 3 times, a bound that some block reaches.
All inputs are finite; a program needn't handle non-finite values.
Results may differ from a plain program's by a relative error of at most 0.013.
The roundings to bfloat16 on the way count: a program that leaves them out, or rounds other values in their place, can miss the bound.
Values may be sent and summed in bfloat16 or wider, within the bound.
A program may use at most 64 MiB of HBM per device.

v0:
```python
import jax
import jax.numpy as jnp
from jax import lax
from jax.sharding import PartitionSpec as P

FF = 4096
epsilon = 1e-06


def scaled_rows(row_data, squares, feature_count, gain_values):
    factor = lax.rsqrt(squares / feature_count + epsilon)
    return (row_data * factor[:, None] * gain_values.astype(jnp.float32)).astype(jnp.bfloat16)


def rounded_wide(matrix):
    return lax.optimization_barrier(matrix.astype(jnp.bfloat16)).astype(jnp.float32)


def shards(
    tokens,
    mix_gain,
    w_query,
    w_key,
    w_value,
    w_igate,
    w_fgate,
    forget_bias,
    w_out,
    mem_state,
    norm_state,
    max_state,
    ffn_gain,
    route_ids,
    route_weights,
    w_gate,
    w_up,
    w_down,
):
    seq_count, model_width = tokens.shape
    local_heads = mem_state.shape[1]
    head_dim = norm_state.shape[1] // local_heads
    tp_count = lax.axis_size("tp")
    tp_at = lax.axis_index("tp")
    ep_count = lax.axis_size("ep")
    own_width = model_width // tp_count
    top_count = route_ids.shape[1]
    block_units = w_down.shape[0]
    span_count = FF // block_units
    experts = ep_count // span_count
    slot_cap = max(2, 3 * seq_count * top_count // (2 * experts))
    residual_in = tokens.astype(jnp.float32)
    normed = scaled_rows(residual_in, jnp.sum(residual_in * residual_in, 1), model_width, mix_gain)

    def project(weight):
        product = jnp.dot(normed, weight, preferred_element_type=jnp.float32)
        return rounded_wide(product).reshape(seq_count, local_heads, head_dim)

    query_rows = project(w_query)
    key_rows = project(w_key) * head_dim ** (-0.5)
    value_rows = project(w_value)
    head_start = tp_at * local_heads
    input_gate = lax.dynamic_slice_in_dim(
        jnp.dot(normed, w_igate, preferred_element_type=jnp.float32), head_start, local_heads, 1
    )
    forget_pre = jnp.dot(normed, w_fgate, preferred_element_type=jnp.float32) + forget_bias[None, :]
    forget_log = jax.nn.log_sigmoid(
        lax.dynamic_slice_in_dim(forget_pre, head_start, local_heads, 1)
    )
    new_max = jnp.maximum(forget_log + max_state, input_gate)
    keep_weight = jnp.exp(forget_log + max_state - new_max)
    new_weight = jnp.exp(input_gate - new_max)
    memory = mem_state.reshape(seq_count, local_heads, head_dim, head_dim)
    new_memory = (
        keep_weight[:, :, None, None] * memory
        + new_weight[:, :, None, None] * key_rows[:, :, :, None] * value_rows[:, :, None, :]
    )
    new_norm = (
        keep_weight[:, :, None] * norm_state.reshape(seq_count, local_heads, head_dim)
        + new_weight[:, :, None] * key_rows
    )
    numerator = jnp.einsum("shd,shde->she", query_rows, new_memory, precision=lax.Precision.HIGHEST)
    denominator = jnp.sum(query_rows * new_norm, axis=2)
    readout = (numerator / jnp.maximum(jnp.abs(denominator), jnp.exp(-new_max))[:, :, None]).astype(
        jnp.bfloat16
    )
    readout = readout.reshape(seq_count, local_heads * head_dim)
    partial_value = jnp.dot(readout, w_out, preferred_element_type=jnp.float32)
    head_total = lax.psum(partial_value.astype(jnp.bfloat16), "tp").astype(jnp.float32)
    residual = (residual_in + head_total).astype(jnp.bfloat16)
    residual_wide = lax.optimization_barrier(residual).astype(jnp.float32)
    outgoing = scaled_rows(
        residual_wide, jnp.sum(residual_wide * residual_wide, 1), model_width, ffn_gain
    )
    own_residual = lax.dynamic_slice_in_dim(residual, tp_at * own_width, own_width, 1)
    flat_ids = route_ids.reshape(-1)
    matches = (flat_ids[:, None] == jnp.arange(experts, dtype=jnp.int32)[None, :]).astype(jnp.int32)
    slot_rank = jnp.sum((jnp.cumsum(matches, 0) - matches) * matches, 1)
    slot_index = (flat_ids * slot_cap + slot_rank).reshape(seq_count, top_count)
    chosen = (
        slot_index[:, :, None] == jnp.arange(experts * slot_cap, dtype=jnp.int32)[None, None, :]
    ).astype(jnp.float32)
    placing = jnp.sum(chosen, 1).astype(jnp.bfloat16)
    mixing = jnp.sum(chosen * route_weights[:, :, None], 1)
    packed = jnp.einsum("sj,sc->jc", placing, outgoing, preferred_element_type=jnp.float32).astype(
        jnp.bfloat16
    )
    packed_width = packed.shape[1]
    outbound = jnp.broadcast_to(
        packed.reshape(experts, 1, slot_cap, packed_width),
        (experts, span_count, slot_cap, packed_width),
    ).reshape(ep_count, slot_cap, packed_width)
    arrived = lax.all_to_all(outbound, "ep", split_axis=0, concat_axis=0, tiled=True)
    sources = arrived.shape[0]
    item_count = arrived.shape[1]
    flat_rows = arrived.reshape(sources * item_count, arrived.shape[2])
    gate_sum = jnp.dot(flat_rows, w_gate, preferred_element_type=jnp.float32)
    up_sum = jnp.dot(flat_rows, w_up, preferred_element_type=jnp.float32)
    hidden = (jax.nn.silu(gate_sum) * up_sum).astype(jnp.bfloat16)
    partial_out = jnp.dot(
        lax.all_gather(hidden, "tp", axis=1, tiled=True), w_down, preferred_element_type=jnp.float32
    )
    returned = lax.all_to_all(
        partial_out.reshape(sources, item_count, w_down.shape[1]).astype(jnp.bfloat16),
        "ep",
        split_axis=0,
        concat_axis=0,
        tiled=True,
    ).astype(jnp.float32)
    results = jnp.sum(returned.reshape(experts, span_count, slot_cap, own_width), 1).reshape(
        experts * slot_cap, own_width
    )
    routed = jnp.dot(
        mixing, results, precision=lax.Precision.HIGHEST, preferred_element_type=jnp.float32
    )
    out_tokens = (own_residual.astype(jnp.float32) + routed).astype(jnp.bfloat16)
    return (
        out_tokens,
        new_memory.reshape(seq_count, local_heads, head_dim * head_dim),
        new_norm.reshape(seq_count, local_heads * head_dim),
        new_max,
    )


def solution(mesh):
    placed = (
        P("ep", None),
        P(),
        P(None, "tp"),
        P(None, "tp"),
        P(None, "tp"),
        P(),
        P(),
        P(),
        P("tp", None),
        P("ep", "tp", None),
        P("ep", "tp"),
        P("ep", "tp"),
        P(),
        P("ep", None),
        P("ep", None),
        P(None, ("ep", "tp")),
        P(None, ("ep", "tp")),
        P("ep", "tp"),
    )
    return jax.shard_map(
        shards,
        mesh=mesh,
        in_specs=placed,
        out_specs=(P("ep", "tp"), P("ep", "tp", None), P("ep", "tp"), P("ep", "tp")),
        check_vma=False,
    )
```

profile of v0, /device:TPU:0, one launch (start us, length us, event | category | flops | bytes accessed | tf_op | source)
XLA Modules:
  0.0 65.1 jit_solution(17769218186569641081)
XLA Ops:
  0.6 0.0 copy-start
  0.6 0.9 %fusion.9 = f32[8]{0:T(128)S(1)} fusion(bf16[8,2048]{1,0:T(8,128)(2,1)} %param.18), kind=kLoop, calls=%fused_computation.25 | loop fusion | flops 49144 | bytes 32800 | tf_op jit(solution)/shard_map/reduce_sum | solution.py:52
  1.6 0.8 %copy.36 = s32[8,2]{1,0:T(8,128)S(1)} copy(s32[8,2]{0,1:T(2,128)} %param.31) | data formatting | bytes 128 | tf_op args[13]
  2.4 0.1 eq.28
  2.4 0.7 %copy.34 = f32[8,1]{1,0:T(8,128)S(1)} copy(f32[8,1]{0,1:T(1,128)} %param.29) | data formatting | bytes 64 | tf_op args[11]
  3.2 0.7 %convert_element_type.78 = f32[2048]{0:T(1024)S(1)} convert(bf16[2048]{0:T(1024)(128)(2,1)} %param.19) | non-fusion elementwise | flops 2048 | bytes 12288 | tf_op jit(solution)/shard_map/convert_element_type | solution.py:12
  3.9 1.3 %convolution_convert_fusion.4 = bf16[8,128]{1,0:T(8,128)(2,1)S(1)} fusion(bf16[2048,128]{1,0:T(8,128)(2,1)} %param.21, bf16[8,2048]{1,0:T(8,128)(2,1)} %param.18, f32[2048]{0:T(1024)S(1)} %convert_element_type.78, f32[8]{0:T(128)S(1)} %add_rsqrt_fusion.1), kind=kOutput, calls=%fused_computation.9 | convolution fusion | flops 4260864 | bytes 567328 | tf_op jit(solution)/shard_map/dot_general | solution.py:55
  5.2 1.3 %convolution_convert_fusion.3 = bf16[8,128]{1,0:T(8,128)(2,1)S(1)} fusion(bf16[2048,128]{1,0:T(8,128)(2,1)} %param.22, bf16[8,2048]{1,0:T(8,128)(2,1)} %param.18, f32[2048]{0:T(1024)S(1)} %convert_element_type.78, f32[8]{0:T(128)S(1)} %add_rsqrt_fusion.1), kind=kOutput, calls=%fused_computation.8 | convolution fusion | flops 4260864 | bytes 567328 | tf_op jit(solution)/shard_map/dot_general | solution.py:55
  6.5 1.3 %convolution_convert_fusion.5 = bf16[8,128]{1,0:T(8,128)(2,1)S(1)} fusion(bf16[2048,128]{1,0:T(8,128)(2,1)} %param.20, bf16[8,2048]{1,0:T(8,128)(2,1)} %param.18, f32[2048]{0:T(1024)S(1)} %convert_element_type.78, f32[8]{0:T(128)S(1)} %add_rsqrt_fusion.1), kind=kOutput, calls=%fused_computation.10 | convolution fusion | flops 4260864 | bytes 567328 | tf_op jit(solution)/shard_map/dot_general | solution.py:55
  7.8 1.0 %fusion.24 = f32[8,4]{1,0:T(8,128)S(1)} fusion(bf16[2048,4]{0,1:T(4,128)(2,1)} %param.23, bf16[8,2048]{1,0:T(8,128)(2,1)} %param.18, f32[2048]{0:T(1024)S(1)} %convert_element_type.78, f32[8]{0:T(128)S(1)} %add_rsqrt_fusion.1), kind=kOutput, calls=%fused_computation.55 | convolution fusion | flops 196608 | bytes 57504 | tf_op jit(solution)/shard_map/dot_general | solution.py:63
  8.7 1.0 %convolution_add_fusion.1 = f32[8,4]{1,0:T(8,128)S(1)} fusion(bf16[2048,4]{0,1:T(4,128)(2,1)} %param.24, f32[4]{0:T(128)} %param.25, bf16[8,2048]{1,0:T(8,128)(2,1)} %param.18, f32[2048]{0:T(1024)S(1)} %convert_element_type.78, f32[8]{0:T(128)S(1)} %add_rsqrt_fusion.1), kind=kOutput, calls=%fused_computation.7 | convolution fusion | flops 196640 | bytes 57520 | tf_op jit(solution)/shard_map/dot_general | solution.py:65
  9.7 0.2 multiply_reduce_fusion.1
  9.9 1.5 %multiply_reduce_fusion = (f32[8]{0:T(128)S(1)}, f32[8,128]{1,0:T(8,128)}, f32[8,128]{1,0:T(8,128)S(1)}) fusion(bf16[8,128]{1,0:T(8,128)(2,1)S(1)} %convolution_convert_fusion.5, f32[8]{0:T(128)S(1)} %get-tuple-element.16, bf16[8,128]{1,0:T(8,128)(2,1)S(1)} %convolution_convert_fusion.4, f32[8,128]{1,0:T(8,128)} %param.28, f32[8]{0:T(128)S(1)} %get-tuple-element.17), kind=kLoop, calls=%fused_computation.44 | loop fusion | flops 7160 | bytes 16480 | tf_op jit(solution)/shard_map/reduce_sum | solution.py:82
  11.4 0.1 copy.35
  11.5 0.1 fusion.16
  11.6 0.2 select_reduce_fusion.1
  11.8 0.1 reduce_sum.63
  11.9 0.1 copy.38
  12.0 0.7 %convert_element_type.95 = f32[2048]{0:T(1024)S(1)} convert(bf16[2048]{0:T(1024)(128)(2,1)} %param.30) | non-fusion elementwise | flops 2048 | bytes 12288 | tf_op jit(solution)/shard_map/convert_element_type | solution.py:12
  12.7 0.1 maximum_reduce_fusion
  12.8 1.5 %fusion.2 = f32[8,1,128]{2,1,0:T(1,128)S(1)} fusion(f32[8,128,128]{2,1,0:T(8,128)} %bitcast.22, f32[8]{0:T(128)S(1)} %get-tuple-element.17, f32[8,128]{1,0:T(8,128)S(1)} %convert_element_type.84, f32[8,128]{1,0:T(8,128)S(1)} %get-tuple-element.23, bf16[8,128,1]{1,0,2:T(8,128)(2,1)S(1)} %bitcast.24), kind=kOutput, calls=%fused_computation.12 | convolution fusion | flops 1966080 | bytes 538656 | tf_op jit(solution)/shard_map/shd,shde->she/dot_general | solution.py:81
  14.3 0.0 copy-done
  14.3 0.2 convolution_convert_fusion.1
  14.5 12.9 %psum.7 = bf16[8,2048]{1,0:T(8,128)(2,1)S(1)} all-reduce(bf16[8,2048]{1,0:T(8,128)(2,1)S(1)} %convolution_convert_fusion.1), channel_id=1, replica_groups=mesh['ep'=8,'tp'=4] {'tp'}, use_global_device_ids=true, to_apply=%region_2.3 | all-reduce | flops 16384 | bytes 65536 | tf_op jit(solution)/shard_map/psum | solution.py:88
  27.5 0.8 %fusion.12 = bf16[8,2048]{1,0:T(8,128)(2,1)S(1)} fusion(bf16[8,2048]{1,0:T(8,128)(2,1)} %param.18, bf16[8,2048]{1,0:T(8,128)(2,1)S(1)} %psum.7), kind=kLoop, calls=%fused_computation.28 | loop fusion | flops 65536 | bytes 98304 | tf_op jit(solution)/shard_map/convert_element_type | solution.py:89
  28.3 0.1 fusion.6
  28.4 0.8 %convert_reduce_fusion = (bf16[8,24]{1,0:T(8,128)(2,1)S(1)}, f32[8,24]{1,0:T(8,128)S(1)}) fusion(s32[8,2]{0,1:T(2,128)S(1)} %copy.38, f32[8,2]{0,1:T(2,128)} %param.32), kind=kLoop, calls=%fused_computation.32 | loop fusion | flops 1536 | bytes 1280 | tf_op jit(solution)/shard_map/reduce_sum | solution.py:102
  29.2 0.2 convolution_convert_fusion
  29.4 0.7 %reshape_reshape.3 = bf16[8,3,2048]{2,1,0:T(4,128)(2,1)} reshape(bf16[24,2048]{1,0:T(8,128)(2,1)S(1)} %convolution_convert_fusion) | data formatting | bytes 196608 | tf_op jit(solution)/shard_map/reshape;reshape | solution.py:111
  30.1 5.8 %all-to-all-start = ((bf16[8,3,2048]{2,1,0:T(4,128)(2,1)}), bf16[8,3,2048]{2,1,0:T(4,128)(2,1)S(1)}, u32[]{:S(2)}, u32[]{:S(2)}) async-start(bf16[8,3,2048]{2,1,0:T(4,128)(2,1)} %reshape_reshape.3), calls=%async_computation | async-start | bytes 262144 | tf_op jit(solution)/shard_map/all_to_all | solution.py:112
  35.9 0.2 broadcast_multiply_fusion
  36.1 7.1 %all-to-all-done = bf16[8,3,2048]{2,1,0:T(4,128)(2,1)S(1)} async-done(((bf16[8,3,2048]{2,1,0:T(4,128)(2,1)}), bf16[8,3,2048]{2,1,0:T(4,128)(2,1)S(1)}, u32[]{:S(2)}, u32[]{:S(2)}) %all-to-all-start) | async-done | bytes 98336 | tf_op jit(solution)/shard_map/all_to_all | solution.py:112
  43.3 0.1 reshape.138
  43.4 0.0 copy-start.1
  43.4 0.0 copy-start.2
  43.4 3.0 %fusion.28 = f32[24,1024]{1,0:T(8,128)S(1)} fusion(bf16[24,2048]{1,0:T(8,128)(2,1)S(1)} %reshape.138, bf16[2048,1024]{1,0:T(8,128)(2,1)} %param.33), kind=kOutput, calls=%fused_computation.56 | convolution fusion | flops 100663296 | bytes 4390912 | tf_op jit(solution)/shard_map/dot_general | solution.py:116
  46.4 0.4 copy-done.1
  46.8 0.0 copy-start.3
  46.8 0.7 %fusion = bf16[24,1024]{1,0:T(8,128)(2,1)S(1)} fusion(bf16[24,2048]{1,0:T(8,128)(2,1)S(1)} %reshape.138, bf16[2048,1024]{1,0:T(8,128)(2,1)S(1)} %copy-done.1, f32[24,1024]{1,0:T(8,128)S(1)} %fusion.28), kind=kOutput, calls=%fused_computation.3 | convolution fusion | flops 100810752 | bytes 4440064 | tf_op jit(solution)/shard_map/dot_general | solution.py:117
  47.5 5.6 %all_gather.3 = bf16[24,4096]{1,0:T(8,128)(2,1)S(1)} all-gather(bf16[24,1024]{1,0:T(8,128)(2,1)S(1)} %fusion), channel_id=1, replica_groups=mesh['ep'=8,'tp'=4] {'tp'}, dimensions={1}, use_global_device_ids=true | all-gather | bytes 245760 | tf_op jit(solution)/shard_map/all_gather | solution.py:120
  53.1 0.0 copy-done.2
  53.1 0.7 %convolution_convert_fusion.2 = bf16[24,512]{1,0:T(8,128)(2,1)S(1)} fusion(bf16[24,4096]{1,0:T(8,128)(2,1)S(1)} %all_gather.3, bf16[4096,512]{1,0:T(8,128)(2,1)S(1)} %copy-done.2), kind=kOutput, calls=%fused_computation.4 | convolution fusion | flops 100675584 | bytes 4415488 | tf_op jit(solution)/shard_map/dot_general | solution.py:119
  53.7 0.6 convert_element_type.100
  54.4 3.3 %all-to-all-start.1 = ((bf16[8,3,512]{2,1,0:T(4,128)(2,1)}), bf16[8,3,512]{2,1,0:T(4,128)(2,1)S(1)}, u32[]{:S(2)}, u32[]{:S(2)}) async-start(bf16[8,3,512]{2,1,0:T(4,128)(2,1)} %convert_element_type.100), calls=%async_computation.1 | async-start | bytes 65536 | tf_op jit(solution)/shard_map/all_to_all | solution.py:122
  57.7 0.0 copy-done.3
  57.7 1.4 %multiply_add_fusion = f32[8,1,16384]{2,1,0:T(1,128)} fusion(f32[8,1,16384]{2,1,0:T(1,128)S(1)} %bitcast.23, f32[8,1,16384]{2,1,0:T(1,128)S(1)} %copy-done.3, f32[8]{0:T(128)S(1)} %get-tuple-element.17), kind=kLoop, calls=%fused_computation.11 | loop fusion | flops 262144 | bytes 1572896 | tf_op jit(solution)/shard_map/add | solution.py:74
  59.1 0.6 copy.39
  59.7 4.6 %all-to-all-done.1 = bf16[8,3,512]{2,1,0:T(4,128)(2,1)S(1)} async-done(((bf16[8,3,512]{2,1,0:T(4,128)(2,1)}), bf16[8,3,512]{2,1,0:T(4,128)(2,1)S(1)}, u32[]{:S(2)}, u32[]{:S(2)}) %all-to-all-start.1) | async-done | bytes 24608 | tf_op jit(solution)/shard_map/all_to_all | solution.py:122
  64.4 0.7 %fusion.1 = bf16[8,512]{1,0:T(8,128)(2,1)} fusion(f32[8,24]{1,0:T(8,128)S(1)} %get-tuple-element.19, bf16[24,512]{1,0:T(8,128)(2,1)S(1)} %reshape.139, bf16[8,2048]{1,0:T(8,128)(2,1)S(1)} %fusion.12, s32[]{:T(128)S(6)} %select_n.14), kind=kOutput, calls=%fused_computation.6 | convolution fusion | flops 1191936 | bytes 41732 | tf_op jit(solution)/shard_map/dot_general | solution.py:132
  (7 shorter events, 0.1 us)
Async XLA Ops:
  0.6 13.7 %copy-start = (bf16[128,2048]{1,0:T(8,128)(2,1)S(1)}, bf16[128,2048]{1,0:T(8,128)(2,1)}, u32[]{:S(2)}) copy-start(bf16[128,2048]{1,0:T(8,128)(2,1)} %param.26) | copy-start | bytes 1572868
  30.1 13.1 %all-to-all-start = ((bf16[8,3,2048]{2,1,0:T(4,128)(2,1)}), bf16[8,3,2048]{2,1,0:T(4,128)(2,1)S(1)}, u32[]{:S(2)}, u32[]{:S(2)}) async-start(bf16[8,3,2048]{2,1,0:T(4,128)(2,1)} %reshape_reshape.3), calls=%async_computation | async-start | bytes 262144 | tf_op jit(solution)/shard_map/all_to_all | solution.py:112
  43.4 3.5 %copy-start.1 = (bf16[2048,1024]{1,0:T(8,128)(2,1)S(1)}, bf16[2048,1024]{1,0:T(8,128)(2,1)}, u32[]{:S(2)}) copy-start(bf16[2048,1024]{1,0:T(8,128)(2,1)} %param.34) | copy-start | bytes 12582916
  43.4 9.7 %copy-start.2 = (bf16[4096,512]{1,0:T(8,128)(2,1)S(1)}, bf16[4096,512]{1,0:T(8,128)(2,1)}, u32[]{:S(2)}) copy-start(bf16[4096,512]{1,0:T(8,128)(2,1)} %param.35) | copy-start | bytes 12582916
  46.8 10.9 %copy-start.3 = (f32[8,1,16384]{2,1,0:T(1,128)S(1)}, f32[8,1,16384]{2,1,0:T(1,128)}, u32[]{:S(2)}) copy-start(f32[8,1,16384]{2,1,0:T(1,128)} %param.27) | copy-start | bytes 1572868
  54.4 10.0 %all-to-all-start.1 = ((bf16[8,3,512]{2,1,0:T(4,128)(2,1)}), bf16[8,3,512]{2,1,0:T(4,128)(2,1)S(1)}, u32[]{:S(2)}, u32[]{:S(2)}) async-start(bf16[8,3,512]{2,1,0:T(4,128)(2,1)} %convert_element_type.100), calls=%async_computation.1 | async-start | bytes 65536 | tf_op jit(solution)/shard_map/all_to_all | solution.py:122
where the time goes:
time: 65.9 us; the launch traced here: 65.1 us
  blocking collectives  18.5 us (28%)
  matrix products  12.9 us (20%)
  waiting for transfers between devices  11.8 us (18%)
  starting transfers between devices  9.14 us (14%)
  other arithmetic  7.75 us (12%)
  local copies, waits for them, and re-layouts  4.36 us (7%)
  between operations  0.72 us (1%)
    psum x1, blocking collectives, shards(): lax.psum(partial_value.astype(jnp.bfloat16), 'tp').astype(jnp.float32)  12.9 us
    all_to_all x1, waiting for transfers between devices, shards(): lax.all_to_all(outbound, 'ep', split_axis=0, concat_axis=0, tiled=True)  7.14 us
    all_to_all x1, starting transfers between devices, shards(): lax.all_to_all(outbound, 'ep', split_axis=0, concat_axis=0, tiled=True)  5.8 us
    all_gather x1, blocking collectives, shards(): lax.all_gather(hidden, 'tp', axis=1, tiled=True)  5.59 us
    all_to_all x1, waiting for transfers between devices, shards(): lax.all_to_all(partial_out.reshape(sources, item_count, w_down.shape[1])....  4.63 us
    dot_general x3, matrix products, project(): product = jnp.dot(normed, weight, preferred_element_type=jnp.float32)  3.89 us
    all_to_all x1, starting transfers between devices, shards(): lax.all_to_all(partial_out.reshape(sources, item_count, w_down.shape[1])....  3.33 us
    dot_general x1, matrix products, shards(): gate_sum = jnp.dot(flat_rows, w_gate, preferred_element_type=jnp.float32)  2.99 us
  transfers between devices with their start and end apart: 2, of which 2 were waited for; matrix products, arithmetic and copies ran while one was open for 3% of the time, Pallas kernels for 0%

commit v1 on v0

--- a/solution.py
+++ b/solution.py
@@ -5,6 +5,11 @@
 
 FF = 4096
 epsilon = 1e-06
+
+
+def stack_and_merge(shard, axis, dim):
+    parts = lax.all_gather(shard, axis)
+    return jnp.concatenate(parts, axis=dim)
 
 
 def scaled_rows(row_data, squares, feature_count, gain_values):
@@ -117,7 +122,7 @@
     up_sum = jnp.dot(flat_rows, w_up, preferred_element_type=jnp.float32)
     hidden = (jax.nn.silu(gate_sum) * up_sum).astype(jnp.bfloat16)
     partial_out = jnp.dot(
-        lax.all_gather(hidden, "tp", axis=1, tiled=True), w_down, preferred_element_type=jnp.float32
+        stack_and_merge(hidden, "tp", 1), w_down, preferred_element_type=jnp.float32
     )
     returned = lax.all_to_all(
         partial_out.reshape(sources, item_count, w_down.shape[1]).astype(jnp.bfloat16),

time: 65.9 us -> 68.6 us (1.041)
  matrix products: 12.9 us -> 15 us
    dot_general x1, matrix products: 0.65 us -> 2.84 us  [shards(): jnp.dot(stack_and_merge(hidden, 'tp', 1), w_down, preferred_element_type=...]
    unnamed x11 -> x9, local copies, waits for them, and re-layouts: 2.53 us -> 2.54 us
where the time goes in v1:
time: 68.6 us; the launch traced here: 67.8 us
  blocking collectives  18.7 us (27%)
  matrix products  15 us (22%)
  waiting for transfers between devices  11.8 us (17%)
  starting transfers between devices  9.14 us (13%)
  other arithmetic  7.75 us (11%)
  local copies, waits for them, and re-layouts  4.67 us (7%)
  between operations  0.73 us (1%)
    psum x1, blocking collectives, shards(): lax.psum(partial_value.astype(jnp.bfloat16), 'tp').astype(jnp.float32)  12.9 us
    all_to_all x1, waiting for transfers between devices, shards(): lax.all_to_all(outbound, 'ep', split_axis=0, concat_axis=0, tiled=True)  7.14 us
    all_to_all x1, starting transfers between devices, shards(): lax.all_to_all(outbound, 'ep', split_axis=0, concat_axis=0, tiled=True)  5.81 us
    all_gather x1, blocking collectives, stack_and_merge(): parts = lax.all_gather(shard, axis)  5.73 us
    all_to_all x1, waiting for transfers between devices, shards(): lax.all_to_all(partial_out.reshape(sources, item_count, w_down.shape[1])....  4.63 us
    dot_general x3, matrix products, project(): product = jnp.dot(normed, weight, preferred_element_type=jnp.float32)  3.89 us
    all_to_all x1, starting transfers between devices, shards(): lax.all_to_all(partial_out.reshape(sources, item_count, w_down.shape[1])....  3.33 us
    dot_general x1, matrix products, shards(): gate_sum = jnp.dot(flat_rows, w_gate, preferred_element_type=jnp.float32)  2.99 us
  transfers between devices with their start and end apart: 2, of which 2 were waited for; matrix products, arithmetic and copies ran while one was open for 3% of the time, Pallas kernels for 0%

profile of v1, /device:TPU:0, one launch (start us, length us, event | category | flops | bytes accessed | tf_op | source)
XLA Modules:
  0.0 67.8 jit_solution(8777585695989681386)
XLA Ops:
  0.6 0.0 copy-start
  0.6 0.9 %fusion.15 = f32[8]{0:T(128)S(1)} fusion(bf16[8,2048]{1,0:T(8,128)(2,1)} %param.18), kind=kLoop, calls=%fused_computation.29 | loop fusion | flops 49144 | bytes 32800 | tf_op jit(solution)/shard_map/reduce_sum | solution.py:57
  1.6 0.8 %copy.48 = s32[8,2]{1,0:T(8,128)S(1)} copy(s32[8,2]{0,1:T(2,128)} %param.31) | data formatting | bytes 128 | tf_op args[13]
  2.4 0.1 eq.28
  2.4 0.7 %copy.46 = f32[8,1]{1,0:T(8,128)S(1)} copy(f32[8,1]{0,1:T(1,128)} %param.29) | data formatting | bytes 64 | tf_op args[11]
  3.2 0.7 %convert_element_type.75 = f32[2048]{0:T(1024)S(1)} convert(bf16[2048]{0:T(1024)(128)(2,1)} %param.19) | non-fusion elementwise | flops 2048 | bytes 12288 | tf_op jit(solution)/shard_map/convert_element_type | solution.py:17
  3.9 1.3 %convolution_convert_fusion.3 = bf16[8,128]{1,0:T(8,128)(2,1)S(1)} fusion(bf16[2048,128]{1,0:T(8,128)(2,1)} %param.21, bf16[8,2048]{1,0:T(8,128)(2,1)} %param.18, f32[2048]{0:T(1024)S(1)} %convert_element_type.75, f32[8]{0:T(128)S(1)} %add_rsqrt_fusion.1), kind=kOutput, calls=%fused_computation.11 | convolution fusion | flops 4260864 | bytes 567328 | tf_op jit(solution)/shard_map/dot_general | solution.py:60
  5.2 1.3 %convolution_convert_fusion.2 = bf16[8,128]{1,0:T(8,128)(2,1)S(1)} fusion(bf16[2048,128]{1,0:T(8,128)(2,1)} %param.22, bf16[8,2048]{1,0:T(8,128)(2,1)} %param.18, f32[2048]{0:T(1024)S(1)} %convert_element_type.75, f32[8]{0:T(128)S(1)} %add_rsqrt_fusion.1), kind=kOutput, calls=%fused_computation.10 | convolution fusion | flops 4260864 | bytes 567328 | tf_op jit(solution)/shard_map/dot_general | solution.py:60
  6.5 1.3 %convolution_convert_fusion.4 = bf16[8,128]{1,0:T(8,128)(2,1)S(1)} fusion(bf16[2048,128]{1,0:T(8,128)(2,1)} %param.20, bf16[8,2048]{1,0:T(8,128)(2,1)} %param.18, f32[2048]{0:T(1024)S(1)} %convert_element_type.75, f32[8]{0:T(128)S(1)} %add_rsqrt_fusion.1), kind=kOutput, calls=%fused_computation.12 | convolution fusion | flops 4260864 | bytes 567328 | tf_op jit(solution)/shard_map/dot_general | solution.py:60
  7.8 1.0 %fusion.30 = f32[8,4]{1,0:T(8,128)S(1)} fusion(bf16[2048,4]{0,1:T(4,128)(2,1)} %param.23, bf16[8,2048]{1,0:T(8,128)(2,1)} %param.18, f32[2048]{0:T(1024)S(1)} %convert_element_type.75, f32[8]{0:T(128)S(1)} %add_rsqrt_fusion.1), kind=kOutput, calls=%fused_computation.59 | convolution fusion | flops 196608 | bytes 57504 | tf_op jit(solution)/shard_map/dot_general | solution.py:68
  8.7 1.0 %convolution_add_fusion.1 = f32[8,4]{1,0:T(8,128)S(1)} fusion(bf16[2048,4]{0,1:T(4,128)(2,1)} %param.24, f32[4]{0:T(128)} %param.25, bf16[8,2048]{1,0:T(8,128)(2,1)} %param.18, f32[2048]{0:T(1024)S(1)} %convert_element_type.75, f32[8]{0:T(128)S(1)} %add_rsqrt_fusion.1), kind=kOutput, calls=%fused_computation.9 | convolution fusion | flops 196640 | bytes 57520 | tf_op jit(solution)/shard_map/dot_general | solution.py:70
  9.7 0.2 multiply_reduce_fusion.1
  9.9 1.5 %multiply_reduce_fusion = (f32[8]{0:T(128)S(1)}, f32[8,128]{1,0:T(8,128)}, f32[8,128]{1,0:T(8,128)S(1)}) fusion(bf16[8,128]{1,0:T(8,128)(2,1)S(1)} %convolution_convert_fusion.4, f32[8]{0:T(128)S(1)} %get-tuple-element.20, bf16[8,128]{1,0:T(8,128)(2,1)S(1)} %convolution_convert_fusion.3, f32[8,128]{1,0:T(8,128)} %param.28, f32[8]{0:T(128)S(1)} %get-tuple-element.21), kind=kLoop, calls=%fused_computation.48 | loop fusion | flops 7160 | bytes 16480 | tf_op jit(solution)/shard_map/reduce_sum | solution.py:87
  11.4 0.1 copy.47
  11.5 0.1 fusion.22
  11.6 0.2 select_reduce_fusion.1
  11.8 0.1 reduce_sum.63
  11.9 0.1 copy.50
  12.0 0.7 %convert_element_type.92 = f32[2048]{0:T(1024)S(1)} convert(bf16[2048]{0:T(1024)(128)(2,1)} %param.30) | non-fusion elementwise | flops 2048 | bytes 12288 | tf_op jit(solution)/shard_map/convert_element_type | solution.py:17
  12.7 0.1 maximum_reduce_fusion
  12.8 1.5 %fusion.7 = f32[8,1,128]{2,1,0:T(1,128)S(1)} fusion(f32[8,128,128]{2,1,0:T(8,128)} %bitcast.29, f32[8]{0:T(128)S(1)} %get-tuple-element.21, f32[8,128]{1,0:T(8,128)S(1)} %convert_element_type.81, f32[8,128]{1,0:T(8,128)S(1)} %get-tuple-element.27, bf16[8,128,1]{1,0,2:T(8,128)(2,1)S(1)} %bitcast.33), kind=kOutput, calls=%fused_computation.14 | convolution fusion | flops 1966080 | bytes 538656 | tf_op jit(solution)/shard_map/shd,shde->she/dot_general | solution.py:86
  14.3 0.0 copy-done
  14.3 0.2 convolution_convert_fusion.1
  14.5 12.9 %psum.7 = bf16[8,2048]{1,0:T(8,128)(2,1)S(1)} all-reduce(bf16[8,2048]{1,0:T(8,128)(2,1)S(1)} %convolution_convert_fusion.1), channel_id=1, replica_groups=mesh['ep'=8,'tp'=4] {'tp'}, use_global_device_ids=true, to_apply=%region_2.3 | all-reduce | flops 16384 | bytes 65536 | tf_op jit(solution)/shard_map/psum | solution.py:93
  27.5 0.8 %fusion.18 = bf16[8,2048]{1,0:T(8,128)(2,1)S(1)} fusion(bf16[8,2048]{1,0:T(8,128)(2,1)} %param.18, bf16[8,2048]{1,0:T(8,128)(2,1)S(1)} %psum.7), kind=kLoop, calls=%fused_computation.32 | loop fusion | flops 65536 | bytes 98304 | tf_op jit(solution)/shard_map/convert_element_type | solution.py:94
  28.3 0.1 fusion.12
  28.4 0.8 %convert_reduce_fusion = (bf16[8,24]{1,0:T(8,128)(2,1)S(1)}, f32[8,24]{1,0:T(8,128)S(1)}) fusion(s32[8,2]{0,1:T(2,128)S(1)} %copy.50, f32[8,2]{0,1:T(2,128)} %param.32), kind=kLoop, calls=%fused_computation.36 | loop fusion | flops 1536 | bytes 1280 | tf_op jit(solution)/shard_map/reduce_sum | solution.py:107
  29.2 0.2 convolution_convert_fusion
  29.4 0.7 %reshape_reshape.3 = bf16[8,3,2048]{2,1,0:T(4,128)(2,1)} reshape(bf16[24,2048]{1,0:T(8,128)(2,1)S(1)} %convolution_convert_fusion) | data formatting | bytes 196608 | tf_op jit(solution)/shard_map/reshape;reshape | solution.py:116
  30.1 5.8 %all-to-all-start = ((bf16[8,3,2048]{2,1,0:T(4,128)(2,1)}), bf16[8,3,2048]{2,1,0:T(4,128)(2,1)S(1)}, u32[]{:S(2)}, u32[]{:S(2)}) async-start(bf16[8,3,2048]{2,1,0:T(4,128)(2,1)} %reshape_reshape.3), calls=%async_computation | async-start | bytes 262144 | tf_op jit(solution)/shard_map/all_to_all | solution.py:117
  35.9 0.2 broadcast_multiply_fusion
  36.1 7.1 %all-to-all-done = bf16[8,3,2048]{2,1,0:T(4,128)(2,1)S(1)} async-done(((bf16[8,3,2048]{2,1,0:T(4,128)(2,1)}), bf16[8,3,2048]{2,1,0:T(4,128)(2,1)S(1)}, u32[]{:S(2)}, u32[]{:S(2)}) %all-to-all-start) | async-done | bytes 98336 | tf_op jit(solution)/shard_map/all_to_all | solution.py:117
  43.3 0.1 reshape.143
  43.4 0.0 copy-start.1
  43.4 3.0 %fusion.34 = f32[24,1024]{1,0:T(8,128)S(1)} fusion(bf16[24,2048]{1,0:T(8,128)(2,1)S(1)} %reshape.143, bf16[2048,1024]{1,0:T(8,128)(2,1)} %param.33), kind=kOutput, calls=%fused_computation.60 | convolution fusion | flops 100663296 | bytes 4390912 | tf_op jit(solution)/shard_map/dot_general | solution.py:121
  46.4 0.4 copy-done.1
  46.8 0.7 fusion.2
  47.5 0.0 copy-start.2
  47.5 5.7 %all-gather = bf16[96,1024]{1,0:T(8,128)(2,1)S(1)} all-gather(bf16[24,1024]{1,0:T(8,128)(2,1)S(1)} %fusion.2), channel_id=2, replica_groups=mesh['ep'=8,'tp'=4] {'tp'}, dimensions={0}, use_global_device_ids=true | all-gather | bytes 245760 | tf_op jit(solution)/shard_map/all_gather | solution.py:11
  53.2 0.2 copy.62
  53.4 0.2 dot_general.48
  53.6 2.8 %fusion.3 = bf16[8,3,512]{2,0,1:T(8,128)(2,1)S(1)} fusion(bf16[4096,512]{1,0:T(8,128)(2,1)} %param.35, bf16[8,3,4096]{2,1,0:T(4,128)(2,1)S(1)} %dot_general.48), kind=kOutput, calls=%fused_computation.6 | convolution fusion | flops 100675584 | bytes 4415488 | tf_op jit(solution)/shard_map/dot_general | solution.py:124
  56.4 0.6 copy.53
  57.0 3.3 %all-to-all-start.1 = ((bf16[8,3,512]{2,1,0:T(4,128)(2,1)}), bf16[8,3,512]{2,1,0:T(4,128)(2,1)S(1)}, u32[]{:S(2)}, u32[]{:S(2)}) async-start(bf16[8,3,512]{2,1,0:T(4,128)(2,1)} %copy.53), calls=%async_computation.1 | async-start | bytes 65536 | tf_op jit(solution)/shard_map/all_to_all | solution.py:127
  60.4 0.0 copy-done.2
  60.4 1.4 %multiply_add_fusion = f32[8,1,16384]{2,1,0:T(1,128)} fusion(f32[8,1,16384]{2,1,0:T(1,128)S(1)} %bitcast.30, f32[8,1,16384]{2,1,0:T(1,128)S(1)} %copy-done.2, f32[8]{0:T(128)S(1)} %get-tuple-element.21), kind=kLoop, calls=%fused_computation.13 | loop fusion | flops 262144 | bytes 1572896 | tf_op jit(solution)/shard_map/add | solution.py:79
  61.8 0.6 copy.54
  62.4 4.6 %all-to-all-done.1 = bf16[8,3,512]{2,1,0:T(4,128)(2,1)S(1)} async-done(((bf16[8,3,512]{2,1,0:T(4,128)(2,1)}), bf16[8,3,512]{2,1,0:T(4,128)(2,1)S(1)}, u32[]{:S(2)}, u32[]{:S(2)}) %all-to-all-start.1) | async-done | bytes 24608 | tf_op jit(solution)/shard_map/all_to_all | solution.py:127
  67.0 0.7 %fusion.6 = bf16[8,512]{1,0:T(8,128)(2,1)} fusion(f32[8,24]{1,0:T(8,128)S(1)} %get-tuple-element.23, bf16[24,512]{1,0:T(8,128)(2,1)S(1)} %reshape.145, bf16[8,2048]{1,0:T(8,128)(2,1)S(1)} %fusion.18, s32[]{:T(128)S(6)} %select_n.14), kind=kOutput, calls=%fused_computation.8 | convolution fusion | flops 1191936 | bytes 41732 | tf_op jit(solution)/shard_map/dot_general | solution.py:137
  (7 shorter events, 0.1 us)
Async XLA Ops:
  0.6 13.7 %copy-start = (bf16[128,2048]{1,0:T(8,128)(2,1)S(1)}, bf16[128,2048]{1,0:T(8,128)(2,1)}, u32[]{:S(2)}) copy-start(bf16[128,2048]{1,0:T(8,128)(2,1)} %param.26) | copy-start | bytes 1572868
  30.1 13.1 %all-to-all-start = ((bf16[8,3,2048]{2,1,0:T(4,128)(2,1)}), bf16[8,3,2048]{2,1,0:T(4,128)(2,1)S(1)}, u32[]{:S(2)}, u32[]{:S(2)}) async-start(bf16[8,3,2048]{2,1,0:T(4,128)(2,1)} %reshape_reshape.3), calls=%async_computation | async-start | bytes 262144 | tf_op jit(solution)/shard_map/all_to_all | solution.py:117
  43.4 3.5 %copy-start.1 = (bf16[2048,1024]{1,0:T(8,128)(2,1)S(1)}, bf16[2048,1024]{1,0:T(8,128)(2,1)}, u32[]{:S(2)}) copy-start(bf16[2048,1024]{1,0:T(8,128)(2,1)} %param.34) | copy-start | bytes 12582916
  47.5 12.9 %copy-start.2 = (f32[8,1,16384]{2,1,0:T(1,128)S(1)}, f32[8,1,16384]{2,1,0:T(1,128)}, u32[]{:S(2)}) copy-start(f32[8,1,16384]{2,1,0:T(1,128)} %param.27) | copy-start | bytes 1572868
  57.0 10.0 %all-to-all-start.1 = ((bf16[8,3,512]{2,1,0:T(4,128)(2,1)}), bf16[8,3,512]{2,1,0:T(4,128)(2,1)S(1)}, u32[]{:S(2)}, u32[]{:S(2)}) async-start(bf16[8,3,512]{2,1,0:T(4,128)(2,1)} %copy.53), calls=%async_computation.1 | async-start | bytes 65536 | tf_op jit(solution)/shard_map/all_to_all | solution.py:127
